TPU v7x, 128 devices: a whole 4x4x4 slice. The times are simulated.
128 devices in a mesh: fs: 16 (over z, y), tp: 8 (over x, core).
Axes of the slice: x: 4, y: 4, z: 4, core: 2. Of those that a mesh axis runs over, the one named last changes fastest.
Arguments:
- tokens: bfloat16 [16384, 2048], P(('fs', 'tp')), may hold values from -6 to 6
- norm_gain: float32 [2048], replicated, may hold values from 0.1 to 1.9
- up_weight: float32 [2048, 8192], P('fs', 'tp'), may hold values from -0.125 to 0.125
- down_weight: float32 [8192, 2048], P('tp', 'fs'), may hold values from -0.0625 to 0.0625
Outputs:
- mlp_out: bfloat16 [16384, 2048], P(('fs', 'tp'))
All inputs are finite; a program needn't handle non-finite values.
Results may differ from a plain program's by a relative error of at most 0.0017.
Values may be sent and summed in bfloat16 or wider, within the bound.
A program may use at most 64 MiB of HBM per device.

v0:
```python
import jax
import jax.numpy as jnp
from jax import lax
from jax.sharding import PartitionSpec as P

epsilon = 1e-06


def taken_in(slab, axis, dim, step, start):

    def gathered(part):
        return lax.all_gather(part, axis, axis=dim, tiled=True)

    return step(start, jax.tree.map(gathered, slab), jnp.int32(0))


def on_whole(shard, axis, dim, work):
    return work(lax.all_gather(shard, axis, axis=dim, tiled=True), jnp.int32(0))


def shards(tokens, norm_gain, up_weight, down_weight):
    values = tokens.astype(jnp.float32)
    scale = lax.rsqrt(jnp.mean(values * values, axis=-1, keepdims=True) + epsilon)
    normed = (values * scale * norm_gain).astype(jnp.bfloat16)
    grouped = lax.all_gather(normed, "tp", axis=0, tiled=True)
    empty = jnp.zeros((grouped.shape[0], up_weight.shape[1]), jnp.float32)

    def add_rows(total, piece, start):
        columns = lax.dynamic_slice_in_dim(grouped, start, piece.shape[0], 1)
        return total + jnp.dot(
            columns, piece.astype(jnp.bfloat16), preferred_element_type=jnp.float32
        )

    pre = taken_in(up_weight.astype(jnp.bfloat16), "fs", 0, add_rows, empty)
    hidden = jnp.square(jax.nn.relu(pre)).astype(jnp.bfloat16)

    def project(piece, start):
        return jnp.dot(hidden, piece.astype(jnp.bfloat16), preferred_element_type=jnp.float32)

    terms = on_whole(down_weight.astype(jnp.bfloat16), "fs", 1, project)
    summed = lax.psum_scatter(terms, "tp", scatter_dimension=0, tiled=True)
    return summed.astype(jnp.bfloat16)


def solution(mesh):
    placed = (P(("fs", "tp"), None), P(), P("fs", "tp"), P("tp", "fs"))
    return jax.shard_map(
        shards, mesh=mesh, in_specs=placed, out_specs=P(("fs", "tp"), None), check_vma=False
    )
```

profile of v0, /device:TPU:1, one launch (start us, length us, event | category | flops | bytes accessed | tf_op | source)
XLA Modules:
  0.0 232.5 jit_solution(14041995372060814346)
XLA Ops:
  6.5 0.0 all-gather.4.cloned.1.call-start
  6.5 1.2 fusion
  7.8 2.0 fusion.2
  9.8 0.0 all-gather.4.cloned.1.call-update
  9.8 0.0 all-gather.6.cloned.1.call-start
  9.9 1.8 convert_element_type.20
  11.7 0.0 all-gather.6.cloned.1.call-update
  11.7 0.0 all-gather.8.cloned.1.call-start
  11.7 1.8 convert_element_type.22
  13.5 0.0 all-gather.8.cloned.1.call-update
  13.5 0.0 reduce-scatter.2.cloned.1.call-start
  13.6 32.0 %all-gather.4.cloned.1.call-done = bf16[1024,2048]{1,0:T(8,128)(2,1)} async-done(((bf16[128,2048]{1,0:T(8,128)(2,1)}), bf16[1024,2048]{1,0:T(8,128)(2,1)}) %all-gather.4.cloned.1.call-update) | async-done | bytes 4194320 | tf_op jit(solution)/shard_map/all_gather | solution.py:25
  45.6 53.1 %all-gather.6.cloned.1.call-done = bf16[2048,1024]{1,0:T(8,128)(2,1)} async-done(((bf16[128,1024]{1,0:T(8,128)(2,1)}), bf16[2048,1024]{1,0:T(8,128)(2,1)}) %all-gather.6.cloned.1.call-update) | async-done | bytes 4194320 | tf_op jit(solution)/shard_map/all_gather | solution.py:12
  98.7 57.5 %all-gather.8.cloned.1.call-done = bf16[1024,2048]{1,0:T(8,128)(2,1)} async-done(((bf16[1024,128]{1,0:T(8,128)(2,1)}), bf16[1024,2048]{1,0:T(8,128)(2,1)}) %all-gather.8.cloned.1.call-update) | async-done | bytes 4194320 | tf_op jit(solution)/shard_map/all_gather | solution.py:18
  156.2 15.0 %fusion.3 = f32[1024,2048]{1,0:T(8,128)} fusion(bf16[1024,2048]{1,0:T(8,128)(2,1)} %all-gather.8.cloned.1.call-done, bf16[1024,2048]{1,0:T(8,128)(2,1)} %all-gather.4.cloned.1.call-done, bf16[2048,1024]{1,0:T(8,128)(2,1)} %all-gather.6.cloned.1.call-done), kind=kOutput, calls=%fused_computation.6 | convolution fusion | flops 8593080320 | bytes 20971520 | tf_op jit(solution)/shard_map/dot_general | solution.py:38
  171.2 0.0 reduce-scatter.2.cloned.1.call-update
  171.2 52.6 %reduce-scatter.2.cloned.1.call-done = f32[128,2048]{1,0:T(8,128)} async-done(((f32[1024,2048]{1,0:T(8,128)}), f32[128,2048]{1,0:T(8,128)}) %reduce-scatter.2.cloned.1.call-update) | async-done | bytes 1048592 | tf_op jit(solution)/shard_map/reduce_scatter | solution.py:41
  223.9 2.1 convert_element_type.23
  (1 shorter events, 0.0 us)
Async XLA Ops:
  6.5 39.1 %all-gather.4.cloned.1.call-start = ((), (), s32[]{:S(2)}) async-start(), calls=%async_computation.1 | async-start | bytes 4718592 | tf_op jit(solution)/shard_map/all_gather | solution.py:25
  9.8 88.9 %all-gather.6.cloned.1.call-start = ((), (), s32[]{:S(2)}) async-start(), calls=%async_computation.2 | async-start | bytes 4456448 | tf_op jit(solution)/shard_map/all_gather | solution.py:12
  11.7 144.5 %all-gather.8.cloned.1.call-start = ((), (), s32[]{:S(2)}) async-start(), calls=%async_computation.3 | async-start | bytes 4456448 | tf_op jit(solution)/shard_map/all_gather | solution.py:18
  13.5 210.4 %reduce-scatter.2.cloned.1.call-start = ((), (), s32[]{:S(2)}) async-start(), calls=%async_computation.4 | async-start | bytes 9437184 | tf_op jit(solution)/shard_map/reduce_scatter | solution.py:41
Sparse Core Ops, SparseCore 0:
  9.9 35.6 all-gather.3
  47.7 50.9 all-gather.5
  100.8 55.3 all-gather.7
  171.4 52.4 reduce-scatter.1
where the time goes:
time: 233 us
  waiting for transfers between devices  195 us (84%)
  matrix products  15 us (6%)
  between operations  13.1 us (6%)
  other arithmetic  8.9 us (4%)
    all_gather x1, waiting for transfers between devices, on_whole(): return work(lax.all_gather(shard, axis, axis=dim, tiled=True), jnp.int32(0))  57.5 us
    all_gather x1, waiting for transfers between devices, gathered(): return lax.all_gather(part, axis, axis=dim, tiled=True)  53.1 us
    reduce_scatter x1, waiting for transfers between devices, shards(): summed = lax.psum_scatter(terms, 'tp', scatter_dimension=0, tiled=True)  52.6 us
    all_gather x1, waiting for transfers between devices, shards(): grouped = lax.all_gather(normed, 'tp', axis=0, tiled=True)  32 us
    dot_general x1, matrix products, project(): jnp.dot(hidden, piece.astype(jnp.bfloat16), preferred_element_type=jnp.fl...  15 us
  transfers between devices with their start and end apart: 4, of which 4 were waited for; matrix products, arithmetic and copies ran while one was open for 2% of the time, Pallas kernels for 0%

commit v1 on v0

--- a/solution.py
+++ b/solution.py
@@ -2,6 +2,7 @@
 import jax.numpy as jnp
 from jax import lax
 from jax.sharding import PartitionSpec as P
+from jax.lax import all_to_all, axis_size
 
 epsilon = 1e-06
 
@@ -22,7 +23,14 @@
     values = tokens.astype(jnp.float32)
     scale = lax.rsqrt(jnp.mean(values * values, axis=-1, keepdims=True) + epsilon)
     normed = (values * scale * norm_gain).astype(jnp.bfloat16)
-    grouped = lax.all_gather(normed, "tp", axis=0, tiled=True)
+    width = axis_size("tp")
+    grouped = all_to_all(
+        jnp.tile(normed, [width if m == 0 else 1 for m in range(normed.ndim)]),
+        "tp",
+        split_axis=0,
+        concat_axis=0,
+        tiled=True,
+    )
     empty = jnp.zeros((grouped.shape[0], up_weight.shape[1]), jnp.float32)
 
     def add_rows(total, piece, start):

time: 233 us -> 198 us (0.85)
  waiting for transfers between devices: 195 us -> 107 us
  blocking collectives: 0 us -> 54.3 us
    all_to_all x0 -> x1, blocking collectives: none -> 54.3 us  [shards(): all_to_all(jnp.tile(normed, [width if m == 0 else 1 for m in range(normed...]
    all_gather x1, waiting for transfers between devices: 53.1 us -> 0.01 us  [gathered(): return lax.all_gather(part, axis, axis=dim, tiled=True)]
    all_gather x1 -> x0, waiting for transfers between devices: 32 us -> none  [shards(): grouped = lax.all_gather(normed, 'tp', axis=0, tiled=True)]
    all_gather x1, waiting for transfers between devices: 57.5 us -> 54 us  [on_whole(): return work(lax.all_gather(shard, axis, axis=dim, tiled=True), jnp.int32(0))]
  transfers between devices with their start and end apart: 4 -> 3, of which waited for: 4 -> 2; matrix products, arithmetic and copies ran while one was open for 2% -> 2% of each run, Pallas kernels for 0% -> 0%
where the time goes in v1:
time: 198 us
  waiting for transfers between devices  107 us (54%)
  blocking collectives  54.3 us (27%)
  matrix products  15 us (8%)
  between operations  13.1 us (7%)
  other arithmetic  8.1 us (4%)
    all_to_all x1, blocking collectives, shards(): all_to_all(jnp.tile(normed, [width if m == 0 else 1 for m in range(normed...  54.3 us
    all_gather x1, waiting for transfers between devices, on_whole(): return work(lax.all_gather(shard, axis, axis=dim, tiled=True), jnp.int32(0))  54 us
    reduce_scatter x1, waiting for transfers between devices, shards(): summed = lax.psum_scatter(terms, 'tp', scatter_dimension=0, tiled=True)  52.6 us
    dot_general x1, matrix products, project(): jnp.dot(hidden, piece.astype(jnp.bfloat16), preferred_element_type=jnp.fl...  15 us
  transfers between devices with their start and end apart: 3, of which 2 were waited for; matrix products, arithmetic and copies ran while one was open for 2% of the time, Pallas kernels for 0%

profile of v1, /device:TPU:1, one launch (start us, length us, event | category | flops | bytes accessed | tf_op | source)
XLA Modules:
  0.0 197.8 jit_solution(489317753236248873)
XLA Ops:
  6.5 0.0 all-gather.3.cloned.1.call-start
  6.5 1.8 convert_element_type.20
  8.3 0.0 all-gather.3.cloned.1.call-update
  8.3 0.0 all-gather.5.cloned.1.call-start
  8.4 1.8 convert_element_type.22
  10.2 0.0 all-gather.5.cloned.1.call-update
  10.2 0.0 reduce-scatter.2.cloned.1.call-start
  10.2 1.2 fusion
  11.5 1.2 fusion.2
  12.7 0.5 tile.2
  13.2 54.3 %all_to_all.9 = bf16[8,128,2048]{2,1,0:T(8,128)(2,1)} all-to-all(bf16[8,128,2048]{2,1,0:T(8,128)(2,1)S(1)} %tile.2), channel_id=1, replica_groups=mesh['fs'=16,'tp'=8] {'tp'}, dimensions={0} | all-to-all | bytes 8388608 | tf_op jit(solution)/shard_map/all_to_all | solution.py:27
  67.6 0.0 all-gather.3.cloned.1.call-done
  67.6 54.0 %all-gather.5.cloned.1.call-done = bf16[1024,2048]{1,0:T(8,128)(2,1)} async-done(((bf16[1024,128]{1,0:T(8,128)(2,1)}), bf16[1024,2048]{1,0:T(8,128)(2,1)}) %all-gather.5.cloned.1.call-update) | async-done | bytes 4194320 | tf_op jit(solution)/shard_map/all_gather | solution.py:19
  121.6 15.0 %fusion.3 = f32[1024,2048]{1,0:T(8,128)} fusion(bf16[1024,2048]{1,0:T(8,128)(2,1)} %all-gather.5.cloned.1.call-done, bf16[1024,2048]{1,0:T(8,128)(2,1)} %bitcast.4, bf16[2048,1024]{1,0:T(8,128)(2,1)} %all-gather.3.cloned.1.call-done), kind=kOutput, calls=%fused_computation.6 | convolution fusion | flops 8593080320 | bytes 20971520 | tf_op jit(solution)/shard_map/dot_general | solution.py:46
  136.6 0.0 reduce-scatter.2.cloned.1.call-update
  136.6 52.6 %reduce-scatter.2.cloned.1.call-done = f32[128,2048]{1,0:T(8,128)} async-done(((f32[1024,2048]{1,0:T(8,128)}), f32[128,2048]{1,0:T(8,128)}) %reduce-scatter.2.cloned.1.call-update) | async-done | bytes 1048592 | tf_op jit(solution)/shard_map/reduce_scatter | solution.py:49
  189.2 2.1 %convert_element_type.23 = bf16[128,2048]{1,0:T(8,128)(2,1)} convert(f32[128,2048]{1,0:T(8,128)} %reduce-scatter.2.cloned.1.call-done) | non-fusion elementwise | flops 262144 | bytes 1572864 | tf_op jit(solution)/shard_map/convert_element_type | solution.py:50
  (1 shorter events, 0.0 us)
Async XLA Ops:
  6.5 61.0 %all-gather.3.cloned.1.call-start = ((), (), s32[]{:S(2)}) async-start(), calls=%async_computation.2 | async-start | bytes 4456448 | tf_op jit(solution)/shard_map/all_gather | solution.py:13
  8.3 113.2 %all-gather.5.cloned.1.call-start = ((), (), s32[]{:S(2)}) async-start(), calls=%async_computation.3 | async-start | bytes 4456448 | tf_op jit(solution)/shard_map/all_gather | solution.py:19
  10.2 179.1 %reduce-scatter.2.cloned.1.call-start = ((), (), s32[]{:S(2)}) async-start(), calls=%async_computation.4 | async-start | bytes 9437184 | tf_op jit(solution)/shard_map/reduce_scatter | solution.py:49
Sparse Core Ops, SparseCore 0:
  9.5 54.5 all-gather.2
  66.2 55.3 all-gather.4
  136.7 52.4 reduce-scatter.1
